TPU v7x, 32 devices: a whole 2x2x4 slice. The times are simulated.
32 devices in a mesh: rep: 4 (over y, x), fs: 2 (over core), tp: 4 (over z).
Axes of the slice: x: 2, y: 2, z: 4, core: 2. Of those that a mesh axis runs over, the one named last changes fastest.
Arguments:
- layer_input: bfloat16 [10240, 2048], P(('rep', 'fs'), 'tp'), may hold values from -6 to 6
- cotangent: bfloat16 [10240, 2048], P(('rep', 'fs'), 'tp'), may hold values from -8 to 8
- gate_pre: bfloat16 [10240, 3072], P('rep', 'fs'), may hold values from -8 to 8
- up_pre: bfloat16 [10240, 3072], P('rep', 'fs'), may hold values from -6 to 6
- gate_weight: bfloat16 [2048, 3072], P('tp', 'fs'), may hold values from -0.125 to 0.125
- up_weight: bfloat16 [2048, 3072], P('tp', 'fs'), may hold values from -0.125 to 0.125
- down_weight: bfloat16 [3072, 2048], P('fs', 'tp'), may hold values from -0.109375 to 0.109375
Outputs:
- input_grad: bfloat16 [10240, 2048], P(('rep', 'fs'), 'tp')
- gate_grad: float32 [2048, 3072], P('tp', 'fs')
- up_grad: float32 [2048, 3072], P('tp', 'fs')
- down_grad: float32 [3072, 2048], P('fs', 'tp')
- gate_rows_sq: float32 [2048], P('tp')
- up_rows_sq: float32 [2048], P('tp')
- down_rows_sq: float32 [3072], P('fs')
All inputs are finite; a program needn't handle non-finite values.
Results may differ from a plain program's by a relative error of at most 0.019.
Values may be sent and summed in bfloat16 or wider, within the bound.
A program may use at most 128 MiB of HBM per device.

v0:
```python
import functools
import math

import jax
import jax.numpy as jnp
from jax import lax
from jax.experimental import pallas as pl
from jax.experimental.pallas import tpu as pltpu
from jax.sharding import PartitionSpec as P

MESH = pl.DeviceIdType.MESH
F32 = jnp.float32
BF16 = jnp.bfloat16


def dot(left_side, right_side, left_dim, right_dim):
    return lax.dot_general(
        left_side,
        right_side,
        (((left_dim,), (right_dim,)), ((), ())),
        preferred_element_type=F32,
    )


def fold(values):
    values = values.astype(F32)
    squares = values * values
    return sum(squares[:, at : at + 128] for at in range(0, values.shape[1], 128))


def row_sums(folded):
    return jnp.sum(folded.T, axis=0, keepdims=True)


class Sum:
    def __init__(self, acc, out, row, rows, cols, swap, stage, first, second, full, sems, at):
        self.acc, self.out, self.cols, self.sems, self.at = acc, out, cols, sems, at
        self.stage, self.first, self.second, self.full = stage, first, second, full
        self.all = pl.ds(row, rows)
        rep = lax.axis_index("rep")
        low, high = rep % 2, rep // 2
        to_low, to_high = rep + 1 - 2 * low, rep + 2 - 4 * high
        self.near, self.far = (to_high, to_low) if swap else (to_low, to_high)
        mine, other = (high, low) if swap else (low, high)
        self.half, self.part = rows // 2, rows // 4
        self.mine, self.other = mine, other
        self.keep = row + mine * self.half
        self.give = row + (1 - mine) * self.half

    def copy(self, which, source, target, rep):
        return pltpu.make_async_remote_copy(
            source,
            target,
            self.sems.at[0, self.at, which],
            self.sems.at[1, self.at, which],
            device_id={"rep": rep},
            device_id_type=MESH,
        )

    def rows(self, start, count):
        return pl.ds(pl.multiple_of(start, self.part), count)

    def place(self, flip):
        part = self.keep + (1 - self.other if flip else self.other) * self.part
        return self.full.at[self.rows(part, self.part), self.cols]

    def hop(self, which):
        cols = self.cols
        if which == 0:
            return self.copy(0, self.stage.at[:, cols], self.first.at[:, cols], self.near)
        if which == 1:
            return self.copy(1, self.second.at[0, :, cols], self.second.at[1, :, cols], self.far)
        if which == 4:
            return self.copy(4, self.place(True), self.place(True), self.near)
        to = self.far if which == 2 else self.near
        return self.copy(which, self.place(False), self.place(False), to)

    def local(self):
        here = (self.all, self.cols)
        return pltpu.make_async_copy(
            self.full.at[here], self.out.at[here], self.sems.at[0, self.at, 5]
        )

    def start(self):
        self.stage[:, self.cols] = self.acc[self.rows(self.give, self.half), self.cols].astype(BF16)
        self.hop(0).start()

    def middle(self):
        part, cols = self.part, self.cols
        self.hop(0).wait_recv()
        other = self.first[self.rows((1 - self.other) * part, part), cols].astype(F32)
        given = self.acc[self.rows(self.keep + (1 - self.other) * part, part), cols] + other
        self.second[0, :, cols] = given.astype(BF16)
        self.hop(1).start()

    def finish(self):
        part, cols = self.part, self.cols
        self.hop(1).wait_recv()
        total = self.acc[self.rows(self.keep + self.other * part, part), cols]
        total = total + self.first[self.rows(self.other * part, part), cols].astype(F32)
        total = total + self.second[1, :, cols].astype(F32)
        self.full[self.rows(self.keep + self.other * part, part), cols] = total.astype(BF16)
        self.hop(2).start()
        self.hop(3).start()

    def forward(self):
        self.hop(2).wait_recv()
        self.hop(4).start()

    def collect(self):
        self.hop(3).wait_recv()
        self.hop(4).wait_recv()
        self.local().start()

    def drain(self):
        for which in range(5):
            self.hop(which).wait_send()
        self.local().wait()


def kernel(
    sizes,
    inputs_hbm,
    cot_hbm,
    gate_hbm,
    up_hbm,
    gate_w_hbm,
    up_w_hbm,
    down_w_hbm,
    input_out,
    gate_out,
    up_out,
    down_out,
    rows_out,
    down_rows_out,
    cot,
    down_w,
    inputs,
    gate_w,
    up_w,
    gate_acc,
    up_acc,
    down_acc,
    gate_buf,
    up_buf,
    gate_delta,
    up_delta,
    partial,
    partial_in,
    input_fin,
    gate_stage,
    gate_first,
    gate_second,
    gate_full,
    up_stage,
    up_first,
    up_second,
    up_full,
    down_stage,
    down_first,
    down_second,
    down_full,
    folded,
    squares,
    down_squares,
    load_sem,
    buf_sem,
    line_recv,
    line_right,
    line_left,
    pair_send,
    pair_recv,
    own_sem,
    weight_recv,
    weight_send,
    peer_sem,
    part_send,
    part_recv,
    sum_sem,
    out_sem,
    square_sem,
    down_square_sem,
):
    tps, slabs, side, width, hidden, block, ahead, scale = sizes
    tokens = 2 * side
    rep, fs, tp = lax.axis_index("rep"), lax.axis_index("fs"), lax.axis_index("tp")
    pair = 1 - fs
    low, high = rep % 2, rep // 2
    peers = [rep + 1 - 2 * low, rep + 2 - 4 * high, 3 - rep]
    quarter, half = hidden // 4, hidden // 8

    barrier = pltpu.get_barrier_semaphore()

    def greet(where):
        pl.semaphore_signal(barrier, 1, device_id=where, device_id_type=MESH)

    greet({"fs": pair})
    for peer in peers:
        greet({"rep": peer})

    for by in range(1, tps):
        greet({"tp": (tp + by) % tps})
    pl.semaphore_wait(barrier, 3 + tps)

    def lanes(origin):
        return pl.ds(pl.multiple_of(origin * width, width), width)

    def remote(source, target, send, recv, where):
        return pltpu.make_async_remote_copy(
            source, target, send, recv, device_id=where, device_id_type=MESH
        )

    def weight_slot(origin, group):
        rows = pl.ds(pl.multiple_of(group * quarter, quarter), quarter)
        return down_w.at[rows, lanes(origin)]

    def weight_line(origin, to, side_at, own):
        rows = pl.ds(pl.multiple_of(rep * quarter, quarter), quarter)
        source = down_w_hbm.at[rows] if own else weight_slot(origin, rep)
        return remote(
            source,
            weight_slot(origin, rep),
            weight_send.at[side_at, origin],
            weight_recv.at[origin],
            {"tp": to},
        )

    def weight_half(origin, group, late):
        rows = pl.ds(pl.multiple_of(group * quarter + late * half, half), half)
        return down_w.at[rows, lanes(origin)]

    def weight_peer(origin, at):
        if at < 2:
            place = weight_slot(origin, rep)
        else:
            place = weight_half(origin, peers[at - 2], at - 2)
        to = peers[at % 2 if at < 2 else 3 - at]
        return remote(
            place, place, peer_sem.at[0, origin, at], peer_sem.at[1, origin, at], {"rep": to}
        )

    def weight_from(origin, at):
        if at < 2:
            place = weight_slot(origin, peers[at])
        else:
            place = weight_half(origin, peers[2], at - 2)
        return remote(
            place, place, peer_sem.at[0, origin, at], peer_sem.at[1, origin, at], {"rep": peers[0]}
        )

    def weight_relay(k):
        for origin, inside in ((tp - k, tp >= k), (tp + k, tp + k < tps)):

            @pl.when(inside)
            def _():
                for at in range(2):
                    weight_from(origin, at).wait_recv()
                    weight_peer(origin, at + 2).start()

    def weight_own():
        @pl.when(tp < tps - 1)
        def _():
            weight_line(tp, tp + 1, 0, True).start()

        @pl.when(tp > 0)
        def _():
            weight_line(tp, tp - 1, 1, True).start()

    def weight_step(k):
        origin = tp - k

        @pl.when(origin >= 0)
        def _():
            weight_line(origin, tp, 0, False).wait_recv()

            @pl.when(tp < tps - 1)
            def _():
                weight_line(origin, tp + 1, 0, False).start()

            for at in range(2):
                weight_peer(origin, at).start()

        back = tp + k

        @pl.when(back < tps)
        def _():
            weight_line(back, tp, 1, False).wait_recv()

            @pl.when(tp > 0)
            def _():
                weight_line(back, tp - 1, 1, False).start()

            for at in range(2):
                weight_peer(back, at).start()

    def slot(origin, slab):
        return cot.at[slab, fs, :, lanes(origin)]

    def line(origin, slab, to, sems, own=False):
        source = cot_hbm.at[slab] if own else slot(origin, slab)
        return remote(
            source, slot(origin, slab), sems.at[origin], line_recv.at[origin, slab], {"tp": to}
        )

    def across(origin, slab):
        place = slot(origin, slab)
        return remote(
            place, place, pair_send.at[origin], pair_recv.at[origin, slab], {"fs": pair}
        )

    def send_own(slab):
        @pl.when(tp < tps - 1)
        def _():
            line(tp, slab, tp + 1, line_right, True).start()

        @pl.when(tp > 0)
        def _():
            line(tp, slab, tp - 1, line_left, True).start()

    def forward(step):
        for k in range(1, tps):
            slab = step - k + 1
            inside = jnp.logical_and(slab >= 0, slab < slabs)
            origin = tp - k

            @pl.when(jnp.logical_and(inside, origin >= 0))
            def _():
                line(origin, slab, tp, line_right).wait_recv()

                @pl.when(tp < tps - 1)
                def _():
                    line(origin, slab, tp + 1, line_right).start()

                across(origin, slab).start()

            back = tp + k

            @pl.when(jnp.logical_and(inside, back < tps))
            def _():
                line(back, slab, tp, line_left).wait_recv()

                @pl.when(tp > 0)
                def _():
                    line(back, slab, tp - 1, line_left).start()

                across(back, slab).start()

        @pl.when(step + 2 < slabs)
        def _():
            send_own(step + 2)

    weight_own()
    own_cot = remote(cot_hbm, cot.at[:, fs, :, lanes(tp)], own_sem.at[0], own_sem.at[1], {"fs": pair})
    own_cot.start()
    own_inputs = remote(inputs_hbm, inputs.at[:, fs], own_sem.at[2], own_sem.at[3], {"fs": pair})
    own_inputs.start()

    loads = [
        pltpu.make_async_copy(cot_hbm, cot.at[:, fs, :, lanes(tp)], load_sem.at[0]),
        pltpu.make_async_copy(inputs_hbm, inputs.at[:, fs], load_sem.at[1]),
        pltpu.make_async_copy(down_w_hbm, down_w.at[:, lanes(tp)], load_sem.at[2]),
        pltpu.make_async_copy(gate_w_hbm, gate_w, load_sem.at[3]),
        pltpu.make_async_copy(up_w_hbm, up_w, load_sem.at[4]),
    ]

    def fetch(slab):
        return [
            pltpu.make_async_copy(gate_hbm.at[:, slab], gate_buf.at[slab % 2], buf_sem.at[0, slab % 2]),
            pltpu.make_async_copy(up_hbm.at[:, slab], up_buf.at[slab % 2], buf_sem.at[1, slab % 2]),
        ]

    for copy in fetch(0):
        copy.start()
    for copy in loads:
        copy.start()
    send_own(0)

    def arrive(slab, following):
        for copy in fetch(slab):
            copy.wait()

        @pl.when(following < slabs)
        def _():
            for copy in fetch(following):
                copy.start()

    def saved(slab, cols):
        shape = (tokens, block)
        gate = gate_buf[slab % 2, :, :, cols].reshape(shape).astype(F32)
        up = up_buf[slab % 2, :, :, cols].reshape(shape).astype(F32)
        return gate, up, jax.nn.sigmoid(gate)

    def blocks(body):
        def one(at, carry):
            body(pl.ds(pl.multiple_of(at * block, block), block), at)
            return carry

        lax.fori_loop(0, hidden // block, one, 0)

    gate_acc[...] = jnp.zeros_like(gate_acc)
    up_acc[...] = jnp.zeros_like(up_acc)
    down_acc[...] = jnp.zeros_like(down_acc)
    loads[0].wait()
    own_cot.wait_recv()

    def down_slab(slab, carry):
        arrive(slab, slab + 1)

        def body(cols, at):
            gate, up, sig = saved(slab, cols)
            act = (gate * sig * up).astype(BF16)
            here = cot[slab, :, :, lanes(tp)].reshape(tokens, width)
            down_acc[cols, :] += dot(act, here, 0, 0) * scale

        blocks(body)
        return carry

    first_part = max(1, (slabs * 6) // 10)
    lax.fori_loop(0, first_part, down_slab, 0)
    weight_step(1)
    send_own(1)
    lax.fori_loop(first_part, slabs, down_slab, 0)
    for copy in fetch(0):
        copy.start()

    rest = hidden // 2
    sums_down = [
        Sum(
            down_acc,
            down_out,
            at * rest,
            rest,
            pl.ds(0, width),
            at == 1,
            down_stage.at[at],
            down_first.at[at],
            down_second.at[at],
            down_full,
            sum_sem,
            at,
        )
        for at in range(2)
    ]
    for copy in loads[1:]:
        copy.wait()
    for k in range(2, tps):
        weight_step(k)
        forward(k - 2)
        weight_relay(k - 1)
    weight_relay(tps - 1)
    for one in sums_down:
        one.start()
    own_inputs.wait_recv()
    for step in range(tps - 2, tps - 2 + ahead):
        forward(step)

    for origin in range(tps):

        @pl.when(tp != origin)
        def _():
            for at in range(2, 4):
                weight_from(origin, at).wait_recv()

    def input_part(slab):
        part = dot(gate_delta[...], gate_w[...], 1, 1) + dot(up_delta[...], up_w[...], 1, 1)
        partial[slab] = part.astype(BF16).reshape(2, side, width)
        give(slab).start()

    def give(slab):
        return remote(
            partial.at[slab, pair],
            partial_in.at[slab],
            part_send.at[0],
            part_recv.at[slab],
            {"fs": pair},
        )

    def input_sum(slab):
        give(slab).wait_recv()
        total = partial[slab, fs].astype(F32) + partial_in[slab].astype(F32)
        input_fin[slab] = total.astype(BF16)

    def share(by):
        return remote(
            down_squares.at[tp],
            down_squares.at[tp],
            down_square_sem.at[0, by],
            down_square_sem.at[1, by],
            {"tp": (tp + by) % tps},
        )

    def shared(by):
        origin = (tp + tps - by) % tps
        return remote(
            down_squares.at[origin],
            down_squares.at[origin],
            down_square_sem.at[0, by],
            down_square_sem.at[1, by],
            {"tp": origin},
        )

    def pair_sums(at):
        cols = pl.ds(pl.multiple_of(at * block, block), block)
        refs = [
            (gate_acc, gate_out, False, gate_stage, gate_first, gate_second, gate_full),
            (up_acc, up_out, True, up_stage, up_first, up_second, up_full),
        ]
        return [
            Sum(acc, out, 0, width, cols, swap, *rest, sum_sem, 2 + 2 * at + which)
            for which, (acc, out, swap, *rest) in enumerate(refs)
        ]

    late = slabs - 3

    def main_slab(slab, carry):
        lead = jnp.minimum(jnp.maximum(late - slab, 0), 1) * ahead

        @pl.when(slab != late)
        def _():
            forward(slab + tps - 2 + lead)

        for origin in range(tps):

            @pl.when(tp != origin)
            def _():
                place = cot.at[slab, pair, :, lanes(origin)]
                remote(
                    place,
                    place,
                    pair_send.at[origin],
                    pair_recv.at[origin, slab],
                    {"fs": pair},
                ).wait_recv()

        arrive(slab, slab + 1)
        rows_in = inputs[slab].reshape(tokens, width)

        def body(cols, at):
            grad = dot(cot[slab].reshape(tokens, tps * width), down_w[cols, :], 1, 1)
            gate, up, sig = saved(slab, cols)
            gate_d = (grad * up * sig * (1.0 + gate * (1.0 - sig))).astype(BF16)
            up_d = (grad * (gate * sig)).astype(BF16)
            gate_delta[:, cols] = gate_d
            up_delta[:, cols] = up_d
            gate_acc[:, cols] += dot(rows_in, gate_d, 0, 0) * scale
            up_acc[:, cols] += dot(rows_in, up_d, 0, 0) * scale

            @pl.when(slab == slabs - 1)
            def _():
                for one in pair_sums(at):
                    one.start()

        blocks(body)

        @pl.when(slab < slabs - 1)
        def _():
            input_part(slab)

        @pl.when(slab > 0)
        def _():
            input_sum(slab - 1)

        @pl.when(slab == 1)
        def _():
            for one in sums_down:
                one.middle()

        @pl.when(slab == 2)
        def _():
            for one in sums_down:
                one.finish()

        @pl.when(slab == 4)
        def _():
            for one in sums_down:
                one.forward()

        @pl.when(slab == 6)
        def _():
            for one in sums_down:
                one.collect()
            for at in range(hidden // 128):
                values = fold(down_full[at * 128 : at * 128 + 128, :])
                down_squares[tp, at : at + 1, :] = row_sums(values)
            for by in range(1, tps):
                share(by).start()

        return carry

    lax.fori_loop(0, slabs, main_slab, 0)

    sums = [one for at in range(hidden // block) for one in pair_sums(at)]
    input_part(slabs - 1)
    for one in sums:
        one.middle()
    input_sum(slabs - 1)
    out_copy = pltpu.make_async_copy(input_fin, input_out, out_sem.at[0])
    out_copy.start()
    for one in sums:
        one.finish()
    for by in range(1, tps):
        shared(by).wait_recv()
    down_squares[tps] = sum(down_squares[at] for at in range(tps))
    down_rows_copy = pltpu.make_async_copy(down_squares.at[tps], down_rows_out, out_sem.at[1])
    down_rows_copy.start()
    for by in range(1, tps):
        share(by).wait_send()
    for one in sums:
        one.forward()

    for at in range(hidden // block):
        cols = pl.ds(at * block, block)
        for which, one in enumerate(sums[2 * at : 2 * at + 2]):
            one.collect()
            values = fold(one.full[:, cols])
            folded[which] = values if at == 0 else folded[which] + values
    blocks_in = width // 128
    for which in range(2):
        for at in range(blocks_in):
            row = which * blocks_in + at
            squares[0, row : row + 1, :] = row_sums(folded[which, at * 128 : at * 128 + 128, :])
    swap_squares = remote(
        squares.at[0], squares.at[1], square_sem.at[0], square_sem.at[1], {"fs": pair}
    )
    swap_squares.start()

    own_cot.wait_send()
    own_inputs.wait_send()
    out_copy.wait()

    def sent(origin, sems):
        place = cot.at[:, fs, :, lanes(origin)]
        return remote(place, place, sems.at[origin], own_sem.at[1], {"fs": pair})

    for origin in range(tps):

        @pl.when(jnp.logical_and(origin <= tp, tp < tps - 1))
        def _():
            sent(origin, line_right).wait_send()

        @pl.when(jnp.logical_and(origin >= tp, tp > 0))
        def _():
            sent(origin, line_left).wait_send()

        @pl.when(tp != origin)
        def _():
            sent(origin, pair_send).wait_send()

    remote(partial_in, partial_in, part_send.at[0], own_sem.at[1], {"fs": pair}).wait_send()
    for origin in range(tps):

        @pl.when(jnp.logical_and(origin <= tp, tp < tps - 1))
        def _():
            weight_line(origin, tp, 0, False).wait_send()

        @pl.when(jnp.logical_and(origin >= tp, tp > 0))
        def _():
            weight_line(origin, tp, 1, False).wait_send()

        @pl.when(tp != origin)
        def _():
            for at in range(4):
                weight_peer(origin, at).wait_send()

    for one in sums_down + sums:
        one.drain()
    swap_squares.wait()
    squares[2] = squares[0] + squares[1]
    rows_copy = pltpu.make_async_copy(squares.at[2], rows_out, out_sem.at[2])
    rows_copy.start()
    rows_copy.wait()
    down_rows_copy.wait()


def widen_kernel(*refs):
    half = len(refs) // 2
    for source, target in zip(refs[:half], refs[half:]):
        target[...] = source[...].astype(target.dtype)


def widen(values, kinds, steps):
    specs = [pl.BlockSpec((v.shape[0] // steps, v.shape[1]), lambda i: (i, 0)) for v in values]
    return pl.pallas_call(
        widen_kernel,
        grid=(steps,),
        out_shape=[jax.ShapeDtypeStruct(v.shape, kind) for v, kind in zip(values, kinds)],
        in_specs=specs,
        out_specs=specs,
        compiler_params=pltpu.CompilerParams(vmem_limit_bytes=40 * 2**20),
        name="widen",
    )(*values)


def on_device(layer_input, cotangent, gate_pre, up_pre, gate_weight, up_weight, down_weight):
    tps, groups = lax.axis_size("tp"), lax.axis_size("rep")
    rows, width = layer_input.shape
    hidden = gate_pre.shape[1]
    side = math.gcd(rows, 128)
    slabs = rows // side
    block = math.gcd(hidden, 512)
    scale = 1.0 / math.sqrt(rows * groups * lax.axis_size("fs"))
    sizes = (tps, slabs, side, width, hidden, block, 1, scale)
    half, part = width // 2, width // 4
    rest = hidden // 2
    vmem = pltpu.VMEM
    dma = pltpu.SemaphoreType.DMA
    anywhere = pl.BlockSpec(memory_space=pl.ANY)
    pieces = lambda value: value.reshape(slabs, side, value.shape[1])
    both = lambda value: value.reshape(2, slabs, side, value.shape[1])
    sums_of = lambda n: [
        vmem((half, hidden), BF16),
        vmem((half, hidden), BF16),
        vmem((2, part, hidden), BF16),
        vmem((width, hidden), BF16),
    ]
    tokens = 2 * side
    input_grad, gate_grad, up_grad, down_grad, row_squares, down_squares = pl.pallas_call(
        functools.partial(kernel, sizes),
        out_shape=(
            jax.ShapeDtypeStruct((slabs, side, width), BF16),
            jax.ShapeDtypeStruct((width, hidden), BF16),
            jax.ShapeDtypeStruct((width, hidden), BF16),
            jax.ShapeDtypeStruct((hidden, width), BF16),
            jax.ShapeDtypeStruct((2 * width // 128, 128), F32),
            jax.ShapeDtypeStruct((hidden // 128, 128), F32),
        ),
        in_specs=[anywhere] * 7,
        out_specs=(anywhere,) * 6,
        scratch_shapes=[
            vmem((slabs, 2, side, tps * width), BF16),
            vmem((hidden, tps * width), BF16),
            vmem((slabs, 2, side, width), BF16),
            vmem((width, hidden), BF16),
            vmem((width, hidden), BF16),
            vmem((width, hidden), F32),
            vmem((width, hidden), F32),
            vmem((hidden, width), F32),
            vmem((2, 2, side, hidden), BF16),
            vmem((2, 2, side, hidden), BF16),
            vmem((tokens, hidden), BF16),
            vmem((tokens, hidden), BF16),
            vmem((slabs, 2, side, width), BF16),
            vmem((slabs, side, width), BF16),
            vmem((slabs, side, width), BF16),
        ]
        + sums_of(0)
        + sums_of(1)
        + [
            vmem((2, rest // 2, width), BF16),
            vmem((2, rest // 2, width), BF16),
            vmem((2, 2, rest // 4, width), BF16),
            vmem((hidden, width), BF16),
            vmem((2, width, 128), F32),
            vmem((3, 2 * width // 128, 128), F32),
            vmem((tps + 1, hidden // 128, 128), F32),
            dma((5,)),
            dma((2, 2)),
            dma((tps, slabs)),
            dma((tps,)),
            dma((tps,)),
            dma((tps,)),
            dma((tps, slabs)),
            dma((4,)),
            dma((tps,)),
            dma((2, tps)),
            dma((2, tps, 4)),
            dma((1,)),
            dma((slabs,)),
            dma((2, 2 + 2 * (hidden // block), 6)),
            dma((3,)),
            dma((2,)),
            dma((2, tps)),
        ],
        compiler_params=pltpu.CompilerParams(
            collective_id=0, has_side_effects=True, vmem_limit_bytes=62 * 2**20
        ),
        name="backward",
    )(
        pieces(layer_input),
        pieces(cotangent),
        both(gate_pre),
        both(up_pre),
        gate_weight,
        up_weight,
        down_weight,
    )
    input_grad = input_grad.reshape(rows, width)
    input_grad, gate_grad, up_grad, down_grad = widen(
        [input_grad, gate_grad, up_grad, down_grad], [BF16, F32, F32, F32], 4
    )
    squares = row_squares.reshape(2, width)
    return (
        input_grad,
        gate_grad,
        up_grad,
        down_grad,
        squares[0],
        squares[1],
        down_squares.reshape(hidden),
    )


def solution(mesh):
    return jax.shard_map(
        on_device,
        mesh=mesh,
        in_specs=(
            P(("rep", "fs"), "tp"),
            P(("rep", "fs"), "tp"),
            P("rep", "fs"),
            P("rep", "fs"),
            P("tp", "fs"),
            P("tp", "fs"),
            P("fs", "tp"),
        ),
        out_specs=(
            P(("rep", "fs"), "tp"),
            P("tp", "fs"),
            P("tp", "fs"),
            P("fs", "tp"),
            P("tp"),
            P("tp"),
            P("fs"),
        ),
        check_vma=False,
    )
```

profile of v0, /device:TPU:0, one launch (start us, length us, event | category | flops | bytes accessed | tf_op | source)
XLA Modules:
  0.0 196.6 jit_solution(16360575958427495907)
XLA Ops:
  0.6 184.3 %backward.1 = (bf16[10,128,512]{2,1,0:T(8,128)(2,1)}, bf16[512,1536]{1,0:T(8,128)(2,1)}, bf16[512,1536]{1,0:T(8,128)(2,1)}, bf16[1536,512]{1,0:T(8,128)(2,1)}, f32[8,128]{1,0:T(8,128)}, /*index=5*/f32[12,128]{1,0:T(8,128)}) custom-call(bf16[10,128,512]{2,1,0:T(8,128)(2,1)} %bitcast.13, bf16[10,128,512]{2,1,0:T(8,128)(2,1)} %bitcast.14, ...), custom_call_target="tpu_custom_call" | custom-call | tf_op jit(solution)/shard_map/backward/pallas_call | solution.py:717
  185.0 1.3 slice_bitcast_fusion
  186.3 0.0 copy-start
  186.3 1.4 copy-done
  187.7 0.0 copy-start.1
  187.7 1.4 copy-done.1
  189.1 0.0 copy-start.2
  189.1 1.4 copy-done.2
  190.5 0.0 copy-start.3
  190.5 1.3 copy-done.3
  191.9 0.0 copy-start.4
  191.9 4.1 %widen.1 = (bf16[1280,512]{1,0:T(8,128)(2,1)}, f32[512,1536]{1,0:T(8,128)}, f32[512,1536]{1,0:T(8,128)}, f32[1536,512]{1,0:T(8,128)}) custom-call(bf16[1280,512]{1,0:T(8,128)(2,1)S(1)} %bitcast.10, bf16[512,1536]{1,0:T(8,128)(2,1)S(1)} %copy-done, bf16[512,1536]{1,0:T(8,128)(2,1)S(1)} %copy-done.1, bf16[1536,512]{1,0:T(8,128)(2,1)S(1)} %copy-done.2), custom_call_target="tpu_custom_call" | custom-call | tf_op jit(solution)/shard_map/widen/pallas_call | solution.py:683
  196.0 0.0 copy-done.4
  196.0 0.6 copy.15
Async XLA Ops:
  186.3 1.4 copy-start
  187.7 1.4 copy-start.1
  189.1 1.4 copy-start.2
  190.5 1.3 copy-start.3
  191.9 4.1 %copy-start.4 = (f32[12,128]{1,0:T(8,128)S(1)}, f32[12,128]{1,0:T(8,128)}, u32[]{:S(2)}) copy-start(f32[12,128]{1,0:T(8,128)} %get-tuple-element.26) | copy-start | bytes 18436
where the time goes:
time: 197 us
  Pallas kernels  188 us (95%)
  local copies, waits for them, and re-layouts  7.48 us (4%)
    pallas_call x1, Pallas kernels, on_device(): pl.pallas_call(functools.partial(kernel, sizes), out_shape=(jax.ShapeDtyp...  184 us
    unnamed x11, local copies, waits for them, and re-layouts  6.14 us
    pallas_call x1, Pallas kernels, widen(): pl.pallas_call(widen_kernel, grid=(steps,), out_shape=[jax.ShapeDtypeStru...  4.14 us

commit v1 on v0

--- a/solution.py
+++ b/solution.py
@@ -510,7 +510,7 @@
             for which, (acc, out, swap, *rest) in enumerate(refs)
         ]
 
-    late = slabs - 3
+    late = slabs // 2
 
     def main_slab(slab, carry):
         lead = jnp.minimum(jnp.maximum(late - slab, 0), 1) * ahead
@@ -672,23 +672,35 @@
     down_rows_copy.wait()
 
 
-def widen_kernel(*refs):
-    half = len(refs) // 2
-    for source, target in zip(refs[:half], refs[half:]):
+def widen_kernel(grads, squares, down_squares, *outs):
+    for source, target in zip(grads, outs[: len(grads)]):
         target[...] = source[...].astype(target.dtype)
-
-
-def widen(values, kinds, steps):
-    specs = [pl.BlockSpec((v.shape[0] // steps, v.shape[1]), lambda i: (i, 0)) for v in values]
-    return pl.pallas_call(
-        widen_kernel,
+    gate_rows, up_rows, down_rows = outs[len(grads) :]
+
+    @pl.when(pl.program_id(0) == 0)
+    def _():
+        count = gate_rows.shape[0]
+        gate_rows[...] = squares[:count, :]
+        up_rows[...] = squares[count:, :]
+        down_rows[...] = down_squares[...]
+
+
+def widen(grads, kinds, squares, down_squares, steps):
+    tall = [pl.BlockSpec((v.shape[0] // steps, v.shape[1]), lambda i: (i, 0)) for v in grads]
+    whole = lambda shape: pl.BlockSpec(shape, lambda i: (0, 0))
+    split = (squares.shape[0] // 2, squares.shape[1])
+    small = [split, split, down_squares.shape]
+    outs = pl.pallas_call(
+        lambda *refs: widen_kernel(refs[: len(grads)], *refs[len(grads) :]),
         grid=(steps,),
-        out_shape=[jax.ShapeDtypeStruct(v.shape, kind) for v, kind in zip(values, kinds)],
-        in_specs=specs,
-        out_specs=specs,
-        compiler_params=pltpu.CompilerParams(vmem_limit_bytes=40 * 2**20),
+        out_shape=[jax.ShapeDtypeStruct(v.shape, kind) for v, kind in zip(grads, kinds)]
+        + [jax.ShapeDtypeStruct(shape, F32) for shape in small],
+        in_specs=tall + [whole(squares.shape), whole(down_squares.shape)],
+        out_specs=tall + [whole(shape) for shape in small],
+        compiler_params=pltpu.CompilerParams(vmem_limit_bytes=62 * 2**20),
         name="widen",
-    )(*values)
+    )(*grads, squares, down_squares)
+    return [*outs[: len(grads)], *(v.reshape(-1) for v in outs[len(grads) :])]
 
 
 def on_device(layer_input, cotangent, gate_pre, up_pre, gate_weight, up_weight, down_weight):
@@ -785,18 +797,14 @@
         down_weight,
     )
     input_grad = input_grad.reshape(rows, width)
-    input_grad, gate_grad, up_grad, down_grad = widen(
-        [input_grad, gate_grad, up_grad, down_grad], [BF16, F32, F32, F32], 4
-    )
-    squares = row_squares.reshape(2, width)
-    return (
-        input_grad,
-        gate_grad,
-        up_grad,
-        down_grad,
-        squares[0],
-        squares[1],
-        down_squares.reshape(hidden),
+    return tuple(
+        widen(
+            [input_grad, gate_grad, up_grad, down_grad],
+            [BF16, F32, F32, F32],
+            row_squares,
+            down_squares,
+            4,
+        )
     )
 
 

time: 197 us -> 190 us (0.964)
  local copies, waits for them, and re-layouts: 7.48 us -> 0 us
    unnamed x11 -> x0, local copies, waits for them, and re-layouts: 6.14 us -> none
    pallas_call x1, Pallas kernels: 184 us -> 181 us  [on_device(): pl.pallas_call(functools.partial(kernel, sizes), out_shape=(jax.ShapeDtyp...]
    pallas_call x1, Pallas kernels: 4.14 us -> 7.28 us  [widen(): pl.pallas_call(lambda *refs: widen_kernel(refs[:len(grads)], *refs[len(gr...]
where the time goes in v1:
time: 190 us; the launch traced here: 189 us
  Pallas kernels  188 us (99%)
    pallas_call x1, Pallas kernels, on_device(): pl.pallas_call(functools.partial(kernel, sizes), out_shape=(jax.ShapeDtyp...  181 us
    pallas_call x1, Pallas kernels, widen(): pl.pallas_call(lambda *refs: widen_kernel(refs[:len(grads)], *refs[len(gr...  7.28 us

profile of v1, /device:TPU:0, one launch (start us, length us, event | category | flops | bytes accessed | tf_op | source)
XLA Modules:
  0.0 189.1 jit_solution(11292192812474489636)
XLA Ops:
  0.6 181.2 %backward.1 = (bf16[10,128,512]{2,1,0:T(8,128)(2,1)}, bf16[512,1536]{1,0:T(8,128)(2,1)}, bf16[512,1536]{1,0:T(8,128)(2,1)}, bf16[1536,512]{1,0:T(8,128)(2,1)}, f32[8,128]{1,0:T(8,128)}, /*index=5*/f32[12,128]{1,0:T(8,128)}) custom-call(bf16[10,128,512]{2,1,0:T(8,128)(2,1)} %bitcast.10, bf16[10,128,512]{2,1,0:T(8,128)(2,1)} %bitcast.11, ...), custom_call_target="tpu_custom_call" | custom-call | tf_op jit(solution)/shard_map/backward/pallas_call | solution.py:729
  181.8 7.3 %widen.1 = (bf16[1280,512]{1,0:T(8,128)(2,1)}, f32[512,1536]{1,0:T(8,128)}, f32[512,1536]{1,0:T(8,128)}, f32[1536,512]{1,0:T(8,128)}, f32[4,128]{1,0:T(4,128)}, /*index=5*/f32[4,128]{1,0:T(4,128)}, f32[12,128]{1,0:T(8,128)}) custom-call(bf16[1280,512]{1,0:T(8,128)(2,1)} %bitcast.12, bf16[512,1536]{1,0:T(8,128)(2,1)} %get-tuple-element.21.refs_1_, ...), custom_call_target="tpu_custom_call" | custom-call | tf_op jit(solution)/shard_map/widen/pallas_call | solution.py:693
